TPU v7x, 512 devices: a whole 4x8x8 slice. The times are simulated.
512 devices in a mesh: tp: 32 (over z, x), dp: 16 (over y, core).
Axes of the slice: x: 4, y: 8, z: 8, core: 2. Of those that a mesh axis runs over, the one named last changes fastest.
Arguments:
- tokens: bfloat16 [256, 4096], P('dp', 'tp'), may hold values from -6 to 6
- norm_gain: float32 [2, 4096], replicated, may hold values from 0.1 to 1.9
- w_in: bfloat16 [2, 4096, 2048], P(None, 'dp', 'tp'), may hold values from -0.09375 to 0.09375
- w_gate: bfloat16 [2, 4096, 2048], P(None, 'dp', 'tp'), may hold values from -0.1875 to 0.1875
- decay_rate: float32 [2, 128, 64], P(None, 'tp'), may hold values from 0.05 to 2
- frequency: float32 [2, 128, 64], P(None, 'tp'), may hold values from -3 to 3
- log_step: float32 [2, 128], P(None, 'tp'), may hold values from -3 to 0
- map_re: float32 [2, 128, 16, 64], P(None, 'tp'), may hold values from -1.5 to 1.5
- map_im: float32 [2, 128, 16, 64], P(None, 'tp'), may hold values from -1.5 to 1.5
- read_re: float32 [2, 128, 16, 64], P(None, 'tp'), may hold values from -0.5 to 0.5
- read_im: float32 [2, 128, 16, 64], P(None, 'tp'), may hold values from -0.5 to 0.5
- skip_weight: float32 [2, 128, 16], P(None, 'tp'), may hold values from -4 to 4
- w_out: bfloat16 [2, 2048, 4096], P(None, 'dp', 'tp'), may hold values from -0.25 to 0.25
- state_re: float32 [2, 256, 128, 64], P(None, 'dp', 'tp'), may hold values from -6 to 6
- state_im: float32 [2, 256, 128, 64], P(None, 'dp', 'tp'), may hold values from -6 to 6
Outputs:
- hidden: bfloat16 [256, 4096], P('dp', 'tp')
- new_re: float32 [2, 256, 128, 64], P(None, 'dp', 'tp')
- new_im: float32 [2, 256, 128, 64], P(None, 'dp', 'tp')
All inputs are finite; a program needn't handle non-finite values.
Results may differ from a plain program's by a relative error of at most 0.01.
Values may be sent and summed in bfloat16 or wider, within the bound.
No kernel may reach another device: no remote copies, remote signals or barrier semaphores. Data moves between devices by JAX's collectives and lax.ppermute only.
A program may use at most 64 MiB of HBM per device.

v0:
```python
import jax
import jax.numpy as jnp
from jax import lax
from jax.sharding import PartitionSpec as P

EPSILON = 1e-06
HIGH = lax.Precision.HIGHEST


def from_everyone(array, axis):
    copies = jnp.broadcast_to(array, (lax.axis_size(axis), *array.shape))
    return lax.all_to_all(copies, axis, split_axis=0, concat_axis=0, tiled=True)


def laid_out(tiles, dim):
    dims = list(tiles.shape[1:])
    dims[dim] *= tiles.shape[0]
    return jnp.moveaxis(tiles, 0, dim).reshape(dims)


def gather_directly(array, axis, dim):
    tiles = from_everyone(array, axis)
    return laid_out(tiles, dim)


def in_one_piece(arrays, axis, dim, along):
    both = jnp.concatenate(arrays, axis=along)
    out, at, gathered = (lax.all_gather(both, axis, axis=dim, tiled=True), 0, [])
    for a in arrays:
        gathered.append(lax.slice_in_dim(out, at, at + a.shape[along], axis=along))
        at += a.shape[along]
    return tuple(gathered)


def state_update(
    inputs,
    old_re,
    old_im,
    decay_rate,
    frequency,
    log_step,
    map_re,
    map_im,
    read_re,
    read_im,
    skip_weight,
):
    lam_re = -decay_rate
    step_size = jnp.exp(log_step)[:, None]
    magnitude = jnp.exp(lam_re * step_size)
    decay_re = magnitude * jnp.cos(frequency * step_size)
    decay_im = magnitude * jnp.sin(frequency * step_size)
    modulus = lam_re * lam_re + frequency * frequency
    hold_re = ((decay_re - 1.0) * lam_re + decay_im * frequency) / modulus
    hold_im = (decay_im * lam_re - (decay_re - 1.0) * frequency) / modulus
    drive_re = hold_re[:, None, :] * map_re - hold_im[:, None, :] * map_im
    drive_im = hold_re[:, None, :] * map_im + hold_im[:, None, :] * map_re
    push_re = jnp.einsum("bgc,gcn->bgn", inputs, drive_re, precision=HIGH)
    push_im = jnp.einsum("bgc,gcn->bgn", inputs, drive_im, precision=HIGH)
    fresh_re = decay_re * old_re - decay_im * old_im + push_re
    fresh_im = decay_re * old_im + decay_im * old_re + push_im
    readout = (
        jnp.einsum("bgn,gcn->bgc", fresh_re, read_re, precision=HIGH)
        - jnp.einsum("bgn,gcn->bgc", fresh_im, read_im, precision=HIGH)
        + skip_weight * inputs
    )
    return (readout, fresh_re, fresh_im)


def local(
    tokens,
    norm_gain,
    w_in,
    w_gate,
    decay_rate,
    frequency,
    log_step,
    map_re,
    map_im,
    read_re,
    read_im,
    skip_weight,
    w_out,
    state_re,
    state_im,
):
    hidden = tokens
    seq_rows = tokens.shape[0]
    local_cols = w_in.shape[2]
    local_groups = decay_rate.shape[1]
    all_re = []
    all_im = []
    for layer in range(w_in.shape[0]):
        whole = gather_directly(hidden, "tp", 1)
        floats = whole.astype(jnp.float32)
        inv_scale = lax.rsqrt(jnp.mean(floats * floats, axis=-1, keepdims=True) + EPSILON)
        normed = (floats * inv_scale * norm_gain[layer]).astype(jnp.bfloat16)
        pieces = in_one_piece((w_in[layer], w_gate[layer]), "dp", 0, 1)
        drive_sum = jnp.dot(normed, pieces[0], preferred_element_type=jnp.float32)
        gate_sum = jnp.dot(normed, pieces[1], preferred_element_type=jnp.float32)
        projected = drive_sum.astype(jnp.bfloat16)
        gate = gate_sum.astype(jnp.bfloat16)
        inputs = projected.astype(jnp.float32).reshape(seq_rows, local_groups, -1)
        readout, fresh_re, fresh_im = state_update(
            inputs,
            state_re[layer],
            state_im[layer],
            decay_rate[layer],
            frequency[layer],
            log_step[layer],
            map_re[layer],
            map_im[layer],
            read_re[layer],
            read_im[layer],
            skip_weight[layer],
        )
        activated = jax.nn.gelu(readout.reshape(seq_rows, local_cols))
        mixer = (activated * jax.nn.sigmoid(gate.astype(jnp.float32))).astype(jnp.bfloat16)
        full_rows = gather_directly(mixer, "tp", 1)
        mixed = jnp.dot(
            full_rows,
            lax.all_gather(w_out[layer], "dp", axis=0, tiled=True),
            preferred_element_type=jnp.float32,
        )
        hidden = (hidden.astype(jnp.float32) + mixed).astype(jnp.bfloat16)
        all_re.append(fresh_re)
        all_im.append(fresh_im)
    return (hidden, jnp.stack(all_re), jnp.stack(all_im))


def solution(mesh):
    return jax.shard_map(
        local,
        mesh=mesh,
        in_specs=(
            P("dp", "tp"),
            P(),
            P(None, "dp", "tp"),
            P(None, "dp", "tp"),
            P(None, "tp", None),
            P(None, "tp", None),
            P(None, "tp"),
            P(None, "tp", None, None),
            P(None, "tp", None, None),
            P(None, "tp", None, None),
            P(None, "tp", None, None),
            P(None, "tp", None),
            P(None, "dp", "tp"),
            P(None, "dp", "tp", None),
            P(None, "dp", "tp", None),
        ),
        out_specs=(P("dp", "tp"), P(None, "dp", "tp", None), P(None, "dp", "tp", None)),
        check_vma=False,
    )
```

profile of v0, /device:TPU:8, one launch (start us, length us, event | category | flops | bytes accessed | tf_op | source)
XLA Modules:
  0.0 148.4 jit_solution(1583821423735559264)
XLA Ops:
  7.2 0.8 slice_bitcast_fusion.2
  8.0 0.6 pad_maximum_fusion
  8.7 0.7 copy-done.8
  9.4 0.7 broadcast_in_dim.8
  10.0 13.2 %all-to-all-start = ((bf16[32,16,128]{2,1,0:T(8,128)(2,1)}), bf16[32,16,128]{2,1,0:T(8,128)(2,1)S(1)}, u32[]{:S(2)}, u32[]{:S(2)}) async-start(bf16[32,16,128]{2,1,0:T(8,128)(2,1)} %broadcast_in_dim.8), calls=%async_computation | async-start | bytes 262144 | tf_op jit(solution)/shard_map/all_to_all | solution.py:12
  23.2 0.6 pad_maximum_fusion.1
  23.9 0.6 copy-done.12
  24.6 0.1 multiply_bitcast_fusion.3
  24.7 0.1 fusion.94
  24.9 0.5 copy-done.3
  25.4 0.1 copy-done.11
  25.6 0.7 copy-done.4
  26.3 7.4 %all-to-all-done = bf16[32,16,128]{2,1,0:T(8,128)(2,1)S(1)} async-done(((bf16[32,16,128]{2,1,0:T(8,128)(2,1)}), bf16[32,16,128]{2,1,0:T(8,128)(2,1)S(1)}, u32[]{:S(2)}, u32[]{:S(2)}) %all-to-all-start) | async-done | bytes 131104 | tf_op jit(solution)/shard_map/all_to_all | solution.py:12
  33.6 0.1 fusion.30
  33.8 21.3 %all-gather.5.cloned.1.call-done = bf16[4096,128]{0,1:T(8,128)(2,1)} async-done(((bf16[256,128]{0,1:T(8,128)(2,1)}), bf16[4096,128]{0,1:T(8,128)(2,1)}) %all-gather.5.cloned.1.call-update) | async-done | bytes 1048592 | tf_op jit(solution)/shard_map/all_gather | solution.py:28
  55.1 1.4 convolution_convert_fusion.3
  56.5 0.1 reshape.312
  56.6 0.1 fusion.7
  56.7 0.7 copy-done.2
  57.4 0.2 fusion.44
  57.6 0.1 fusion.6
  57.8 0.7 copy-done.6
  58.4 0.2 fusion.5
  58.7 1.4 fusion.21
  60.1 0.8 reshape.326
  60.9 10.1 %all-to-all-start.1 = ((bf16[32,2,512]{2,1,0:T(2,128)(2,1)}), bf16[32,2,512]{2,1,0:T(2,128)(2,1)S(1)}, u32[]{:S(2)}, u32[]{:S(2)}) async-start(bf16[32,2,512]{2,1,0:T(2,128)(2,1)} %reshape.326), calls=%async_computation.1 | async-start | bytes 131072 | tf_op jit(solution)/shard_map/all_to_all | solution.py:12
  71.0 16.1 %all-gather = bf16[1,2048,128]{2,1,0:T(8,128)(2,1)S(1)} all-gather(bf16[1,128,128]{2,1,0:T(8,128)(2,1)S(1)} %get-tuple-element.13), channel_id=2, replica_groups=mesh['tp'=32,'dp'=16] {'dp'}, dimensions={1}, use_global_device_ids=true | all-gather | bytes 557056 | tf_op jit(solution)/shard_map/all_gather | solution.py:122
  87.1 0.1 reshape.327
  87.3 0.2 reshape.315
  87.5 0.2 fusion.22
  87.7 0.7 broadcast_in_dim.10
  88.3 10.2 %all-to-all-start.2 = ((bf16[32,16,128]{2,1,0:T(8,128)(2,1)}), bf16[32,16,128]{2,1,0:T(8,128)(2,1)S(1)}, u32[]{:S(2)}, u32[]{:S(2)}) async-start(bf16[32,16,128]{2,1,0:T(8,128)(2,1)} %broadcast_in_dim.10), calls=%async_computation.2 | async-start | bytes 262144 | tf_op jit(solution)/shard_map/all_to_all | solution.py:12
  98.6 18.5 %all-gather.1 = bf16[1,2048,128]{2,1,0:T(8,128)(2,1)S(1)} all-gather(bf16[1,128,128]{2,1,0:T(8,128)(2,1)S(1)} %get-tuple-element.12), channel_id=3, replica_groups=mesh['tp'=32,'dp'=16] {'dp'}, dimensions={1}, use_global_device_ids=true | all-gather | bytes 557056 | tf_op jit(solution)/shard_map/all_gather | solution.py:122
  117.1 0.1 fusion.31
  117.3 1.4 convolution_convert_fusion.1
  118.8 0.2 fusion.2
  118.9 0.1 fusion.3
  119.1 0.2 fusion.37
  119.3 0.2 fusion.1
  119.6 0.3 fusion.14
  119.9 0.8 reshape.328
  120.7 9.8 %all-to-all-start.3 = ((bf16[32,2,512]{2,1,0:T(2,128)(2,1)}), bf16[32,2,512]{2,1,0:T(2,128)(2,1)S(1)}, u32[]{:S(2)}, u32[]{:S(2)}) async-start(bf16[32,2,512]{2,1,0:T(2,128)(2,1)} %reshape.328), calls=%async_computation.3 | async-start | bytes 131072 | tf_op jit(solution)/shard_map/all_to_all | solution.py:12
  130.5 0.7 copy.62
  131.1 0.7 copy.61
  131.8 8.6 %all-to-all-done.3 = bf16[32,2,512]{2,1,0:T(2,128)(2,1)S(1)} async-done(((bf16[32,2,512]{2,1,0:T(2,128)(2,1)}), bf16[32,2,512]{2,1,0:T(2,128)(2,1)S(1)}, u32[]{:S(2)}, u32[]{:S(2)}) %all-to-all-start.3) | async-done | bytes 65568 | tf_op jit(solution)/shard_map/all_to_all | solution.py:12
  140.4 0.1 reshape.329
  140.6 0.2 reshape.319
  140.8 0.8 fusion.23
  (46 shorter events, 0.8 us)
Async XLA Ops:
  7.2 47.9 %all-gather.5.cloned.1.call-start = ((), (), s32[]{:S(2)}) async-start(), calls=%async_computation.4 | async-start | bytes 1114112 | tf_op jit(solution)/shard_map/all_gather | solution.py:28
  8.7 0.7 copy-start.8
  10.0 23.6 %all-to-all-start = ((bf16[32,16,128]{2,1,0:T(8,128)(2,1)}), bf16[32,16,128]{2,1,0:T(8,128)(2,1)S(1)}, u32[]{:S(2)}, u32[]{:S(2)}) async-start(bf16[32,16,128]{2,1,0:T(8,128)(2,1)} %broadcast_in_dim.8), calls=%async_computation | async-start | bytes 262144 | tf_op jit(solution)/shard_map/all_to_all | solution.py:12
  23.2 94.1 %all-gather.7.cloned.1.call-start = ((), (), s32[]{:S(2)}) async-start(), calls=%async_computation.5 | async-start | bytes 1114112 | tf_op jit(solution)/shard_map/all_gather | solution.py:28
  23.9 0.7 copy-start.12
  23.9 0.7 copy-start.9
  23.9 0.7 copy-start.10
  23.9 1.0 copy-start.7
  24.6 0.8 copy-start.3
  24.9 0.7 copy-start.11
  25.4 0.8 copy-start.4
  25.4 0.9 copy-start.5
  55.1 1.5 copy-start
  55.1 1.5 copy-start.1
  56.6 0.8 copy-start.2
  57.6 0.8 copy-start.6
  60.9 26.2 %all-to-all-start.1 = ((bf16[32,2,512]{2,1,0:T(2,128)(2,1)}), bf16[32,2,512]{2,1,0:T(2,128)(2,1)S(1)}, u32[]{:S(2)}, u32[]{:S(2)}) async-start(bf16[32,2,512]{2,1,0:T(2,128)(2,1)} %reshape.326), calls=%async_computation.1 | async-start | bytes 131072 | tf_op jit(solution)/shard_map/all_to_all | solution.py:12
  88.3 28.7 %all-to-all-start.2 = ((bf16[32,16,128]{2,1,0:T(8,128)(2,1)}), bf16[32,16,128]{2,1,0:T(8,128)(2,1)S(1)}, u32[]{:S(2)}, u32[]{:S(2)}) async-start(bf16[32,16,128]{2,1,0:T(8,128)(2,1)} %broadcast_in_dim.10), calls=%async_computation.2 | async-start | bytes 262144 | tf_op jit(solution)/shard_map/all_to_all | solution.py:12
  117.3 2.3 %copy-start.13 = (bf16[4096,128]{0,1:T(8,128)(2,1)S(1)}, bf16[4096,128]{0,1:T(8,128)(2,1)}, u32[]{:S(2)}) copy-start(bf16[4096,128]{0,1:T(8,128)(2,1)} %all-gather.7.cloned.1.call-done) | copy-start | bytes 3145732
  120.7 19.8 %all-to-all-start.3 = ((bf16[32,2,512]{2,1,0:T(2,128)(2,1)}), bf16[32,2,512]{2,1,0:T(2,128)(2,1)S(1)}, u32[]{:S(2)}, u32[]{:S(2)}) async-start(bf16[32,2,512]{2,1,0:T(2,128)(2,1)} %reshape.328), calls=%async_computation.3 | async-start | bytes 131072 | tf_op jit(solution)/shard_map/all_to_all | solution.py:12
Sparse Core Ops, SparseCore 0:
  10.6 44.4 all-gather.4
  57.7 39.4 all-gather.6
where the time goes:
time: 149 us; the launch traced here: 148 us
  starting transfers between devices  43.4 us (29%)
  waiting for transfers between devices  37.4 us (25%)
  blocking collectives  34.5 us (23%)
  between operations  14.3 us (10%)
  local copies, waits for them, and re-layouts  10.2 us (7%)
  matrix products  6.73 us (5%)
  other arithmetic  1.84 us (1%)
    all_to_all x4, starting transfers between devices, from_everyone(): return lax.all_to_all(copies, axis, split_axis=0, concat_axis=0, tiled=True)  43.3 us
    all_gather x2, blocking collectives, local(): lax.all_gather(w_out[layer], 'dp', axis=0, tiled=True)  34.5 us
    all_gather x2, waiting for transfers between devices, in_one_piece(): lax.all_gather(both, axis, axis=dim, tiled=True)  21.3 us
    all_to_all x4, waiting for transfers between devices, from_everyone(): return lax.all_to_all(copies, axis, split_axis=0, concat_axis=0, tiled=True)  16 us
    unnamed x34, local copies, waits for them, and re-layouts  7.18 us
  transfers between devices with their start and end apart: 6, of which 3 were waited for; matrix products, arithmetic and copies ran while one was open for 6% of the time, Pallas kernels for 0%

commit v1 on v0

--- a/solution.py
+++ b/solution.py
@@ -5,6 +5,28 @@
 
 EPSILON = 1e-06
 HIGH = lax.Precision.HIGHEST
+
+
+def joined_along(pieces, dim):
+    pieces = jnp.moveaxis(pieces, 0, dim)
+    shape = pieces.shape
+    return pieces.reshape(*shape[:dim], shape[dim] * shape[dim + 1], *shape[dim + 2 :])
+
+
+def gather_around(shard, axis, dim):
+    size = lax.axis_size(axis)
+    pairs = [(i, (i + 1) % size) for i in range(size)]
+    back = [(b, a) for a, b in pairs]
+    lower, upper = ([], [])
+    for step in range(size - 1):
+        if step % 2 == 0:
+            lower.append(lax.ppermute(lower[-1] if lower else shard, axis, pairs))
+        else:
+            upper.append(lax.ppermute(upper[-1] if upper else shard, axis, back))
+    blocks = jnp.stack([*lower[::-1], shard, *upper])
+    shift = lax.axis_index(axis) - len(lower)
+    blocks = blocks[(jnp.arange(size) - shift) % size]
+    return joined_along(blocks, dim)
 
 
 def from_everyone(array, axis):
@@ -118,9 +140,7 @@
         mixer = (activated * jax.nn.sigmoid(gate.astype(jnp.float32))).astype(jnp.bfloat16)
         full_rows = gather_directly(mixer, "tp", 1)
         mixed = jnp.dot(
-            full_rows,
-            lax.all_gather(w_out[layer], "dp", axis=0, tiled=True),
-            preferred_element_type=jnp.float32,
+            full_rows, gather_around(w_out[layer], "dp", 0), preferred_element_type=jnp.float32
         )
         hidden = (hidden.astype(jnp.float32) + mixed).astype(jnp.bfloat16)
         all_re.append(fresh_re)

time: 149 us -> 132 us (0.89)
  the two profiles are of different devices: /device:TPU:8 before, /device:TPU:32 now
where the time goes in v1:
time: 132 us; the launch traced here: 131 us
  starting transfers between devices  56.7 us (43%)
  waiting for transfers between devices  40 us (30%)
  between operations  14.6 us (11%)
  local copies, waits for them, and re-layouts  11.4 us (9%)
  matrix products  6.74 us (5%)
  other arithmetic  1.86 us (1%)
    all_to_all x4, starting transfers between devices, from_everyone(): return lax.all_to_all(copies, axis, split_axis=0, concat_axis=0, tiled=True)  30.2 us
    all_to_all x4, waiting for transfers between devices, from_everyone(): return lax.all_to_all(copies, axis, split_axis=0, concat_axis=0, tiled=True)  28.5 us
    ppermute x14, starting transfers between devices, gather_around(): upper.append(lax.ppermute(upper[-1] if upper else shard, axis, back))  26.4 us
    ppermute x16, waiting for transfers between devices, gather_around(): lower.append(lax.ppermute(lower[-1] if lower else shard, axis, pairs))  9.53 us
    unnamed x63, local copies, waits for them, and re-layouts  7 us
    dot_general x2, matrix products, local(): drive_sum = jnp.dot(normed, pieces[0], preferred_element_type=jnp.float32)  2.8 us
  transfers between devices with their start and end apart: 36, of which 17 were waited for; matrix products, arithmetic and copies ran while one was open for 8% of the time, Pallas kernels for 0%

profile of v1, /device:TPU:32, one launch (start us, length us, event | category | flops | bytes accessed | tf_op | source)
XLA Modules:
  0.0 131.3 jit_solution(6057429354853954351)
XLA Ops:
  7.2 0.8 slice_bitcast_fusion.2
  8.0 0.6 pad_maximum_fusion
  8.7 0.8 copy-done
  9.5 2.9 %collective-permute-start.8 = (bf16[128,128]{1,0:T(8,128)(2,1)S(1)}, bf16[128,128]{1,0:T(8,128)(2,1)S(1)}, u32[]{:S(2)}, u32[]{:S(2)}) collective-permute-start(bf16[128,128]{1,0:T(8,128)(2,1)S(1)} %get-tuple-element.15), channel_id=1, source_target_pairs={{1,0},{2,1},{3,2},{4,3},{5,4},{6,5},{7,6},{8,7},{9,8},{10,9},{11,1... | collective-permute-start | bytes 98312 | tf_op jit(solution)/shard_map/ppermute | solution.py:25
  12.5 3.0 %collective-permute-start.23 = (bf16[128,128]{1,0:T(8,128)(2,1)S(1)}, bf16[128,128]{1,0:T(8,128)(2,1)S(1)}, u32[]{:S(2)}, u32[]{:S(2)}) collective-permute-start(bf16[128,128]{1,0:T(8,128)(2,1)S(1)} %get-tuple-element.14), channel_id=1, source_target_pairs={{1,0},{2,1},{3,2},{4,3},{5,4},{6,5},{7,6},{8,7},{9,8},{10,9},{11,1... | collective-permute-start | bytes 98312 | tf_op jit(solution)/shard_map/ppermute | solution.py:25
  15.4 0.7 broadcast_in_dim.8
  16.1 13.2 %all-to-all-start = ((bf16[32,16,128]{2,1,0:T(8,128)(2,1)}), bf16[32,16,128]{2,1,0:T(8,128)(2,1)S(1)}, u32[]{:S(2)}, u32[]{:S(2)}) async-start(bf16[32,16,128]{2,1,0:T(8,128)(2,1)} %broadcast_in_dim.8), calls=%async_computation | async-start | bytes 262144 | tf_op jit(solution)/shard_map/all_to_all | solution.py:34
  29.3 0.6 pad_maximum_fusion.1
  30.1 0.7 copy-done.4
  31.0 0.6 copy-done.12
  31.5 2.4 %collective-permute-start.9 = (bf16[128,128]{1,0:T(8,128)(2,1)S(1)}, bf16[128,128]{1,0:T(8,128)(2,1)S(1)}, u32[]{:S(2)}, u32[]{:S(2)}) collective-permute-start(bf16[128,128]{1,0:T(8,128)(2,1)S(1)} %collective-permute-done.8), channel_id=1, source_target_pairs={{1,0},{2,1},{3,2},{4,3},{5,4},{6,5},{7,6},{8,7},{9,8},{10,9},{11,1... | collective-permute-start | bytes 98312 | tf_op jit(solution)/shard_map/ppermute | solution.py:25
  34.4 1.0 collective-permute-done.1
  35.5 0.5 collective-permute-done.16
  36.1 3.0 %collective-permute-start.10 = (bf16[128,128]{1,0:T(8,128)(2,1)S(1)}, bf16[128,128]{1,0:T(8,128)(2,1)S(1)}, u32[]{:S(2)}, u32[]{:S(2)}) collective-permute-start(bf16[128,128]{1,0:T(8,128)(2,1)S(1)} %collective-permute-done.9), channel_id=1, source_target_pairs={{1,0},{2,1},{3,2},{4,3},{5,4},{6,5},{7,6},{8,7},{9,8},{10,9},{11,1... | collective-permute-start | bytes 98312 | tf_op jit(solution)/shard_map/ppermute | solution.py:25
  39.1 0.5 collective-permute-start.25
  39.6 0.6 collective-permute-done.2
  40.2 0.8 collective-permute-done.17
  41.2 3.0 %collective-permute-start.11 = (bf16[128,128]{1,0:T(8,128)(2,1)S(1)}, bf16[128,128]{1,0:T(8,128)(2,1)S(1)}, u32[]{:S(2)}, u32[]{:S(2)}) collective-permute-start(bf16[128,128]{1,0:T(8,128)(2,1)S(1)} %collective-permute-done.10), channel_id=1, source_target_pairs={{1,0},{2,1},{3,2},{4,3},{5,4},{6,5},{7,6},{8,7},{9,8},{10,9},{11,1... | collective-permute-start | bytes 98312 | tf_op jit(solution)/shard_map/ppermute | solution.py:25
  44.2 0.6 collective-permute-done.3
  44.8 0.8 collective-permute-done.18
  45.9 3.5 %collective-permute-start.12 = (bf16[128,128]{1,0:T(8,128)(2,1)S(1)}, bf16[128,128]{1,0:T(8,128)(2,1)S(1)}, u32[]{:S(2)}, u32[]{:S(2)}) collective-permute-start(bf16[128,128]{1,0:T(8,128)(2,1)S(1)} %collective-permute-done.11), channel_id=1, source_target_pairs={{1,0},{2,1},{3,2},{4,3},{5,4},{6,5},{7,6},{8,7},{9,8},{10,9},{11,1... | collective-permute-start | bytes 98312 | tf_op jit(solution)/shard_map/ppermute | solution.py:25
  49.5 0.6 collective-permute-start.27
  50.2 0.9 collective-permute-done.12
  51.0 3.0 %collective-permute-start.13 = (bf16[128,128]{1,0:T(8,128)(2,1)S(1)}, bf16[128,128]{1,0:T(8,128)(2,1)S(1)}, u32[]{:S(2)}, u32[]{:S(2)}) collective-permute-start(bf16[128,128]{1,0:T(8,128)(2,1)S(1)} %collective-permute-done.12), channel_id=1, source_target_pairs={{1,0},{2,1},{3,2},{4,3},{5,4},{6,5},{7,6},{8,7},{9,8},{10,9},{11,1... | collective-permute-start | bytes 98312 | tf_op jit(solution)/shard_map/ppermute | solution.py:25
  54.0 0.6 collective-permute-start.28
  54.9 0.7 collective-permute-done.13
  55.6 3.0 %collective-permute-start.14 = (bf16[128,128]{1,0:T(8,128)(2,1)S(1)}, bf16[128,128]{1,0:T(8,128)(2,1)S(1)}, u32[]{:S(2)}, u32[]{:S(2)}) collective-permute-start(bf16[128,128]{1,0:T(8,128)(2,1)S(1)} %collective-permute-done.13), channel_id=1, source_target_pairs={{1,0},{2,1},{3,2},{4,3},{5,4},{6,5},{7,6},{8,7},{9,8},{10,9},{11,1... | collective-permute-start | bytes 98312 | tf_op jit(solution)/shard_map/ppermute | solution.py:25
  58.6 0.6 collective-permute-start.29
  59.6 4.0 %collective-permute-done.7 = bf16[128,128]{1,0:T(8,128)(2,1)S(1)} collective-permute-done((bf16[128,128]{1,0:T(8,128)(2,1)S(1)}, bf16[128,128]{1,0:T(8,128)(2,1)S(1)}, u32[]{:S(2)}, u32[]{:S(2)}) %collective-permute-start.7) | collective-permute-done | bytes 32800 | tf_op jit(solution)/shard_map/ppermute | solution.py:23
  64.3 0.6 gather_fusion
  65.0 1.4 %convolution_convert_fusion.3 = bf16[16,64]{1,0:T(8,128)(2,1)S(1)} fusion(bf16[4096,128]{0,1:T(8,128)(2,1)} %all-gather.3.cloned.1.call-done, f32[4096]{0:T(1024)S(1)} %bitcast.358, f32[16]{0:T(128)S(1)} %add_rsqrt_fusion.1, bf16[32,16,128]{2,1,0:T(8,128)(2,1)S(1)} %all-to-all-done), kind=kOutput, calls=%fused_computation.35 | convolution fusion | flops 8651776 | bytes 673856 | tf_op jit(solution)/shard_map/dot_general | solution.py:121
  66.7 0.7 copy-done.3
  67.7 0.7 copy-done.6
  68.7 1.4 %fusion.21 = bf16[16,64]{1,0:T(8,128)(2,1)S(1)} fusion(bf16[4096,128]{0,1:T(8,128)(2,1)} %all-gather.3.cloned.1.call-done, f32[16,64]{1,0:T(8,128)S(1)} %reshape.369, f32[4096]{0:T(1024)S(1)} %bitcast.359, f32[16]{0:T(128)S(1)} %add_rsqrt_fusion.1, bf16[32,16,128]{2,1,0:T(8,128)(2,1)S(1)} %all-to-all-done), kind=kOutput, calls=%fused_computation.34 | convolution fusion | flops 8666112 | bytes 677952 | tf_op jit(solution)/shard_map/dot_general | solution.py:122
  70.1 0.8 reshape.397
  70.8 9.3 %all-to-all-start.1 = ((bf16[32,2,512]{2,1,0:T(2,128)(2,1)}), bf16[32,2,512]{2,1,0:T(2,128)(2,1)S(1)}, u32[]{:S(2)}, u32[]{:S(2)}) async-start(bf16[32,2,512]{2,1,0:T(2,128)(2,1)} %reshape.397), calls=%async_computation.1 | async-start | bytes 131072 | tf_op jit(solution)/shard_map/all_to_all | solution.py:34
  80.2 10.0 %all-to-all-done.1 = bf16[32,2,512]{2,1,0:T(2,128)(2,1)S(1)} async-done(((bf16[32,2,512]{2,1,0:T(2,128)(2,1)}), bf16[32,2,512]{2,1,0:T(2,128)(2,1)S(1)}, u32[]{:S(2)}, u32[]{:S(2)}) %all-to-all-start.1) | async-done | bytes 65568 | tf_op jit(solution)/shard_map/all_to_all | solution.py:34
  90.7 0.7 broadcast_in_dim.10
  91.4 3.9 %all-to-all-start.2 = ((bf16[32,16,128]{2,1,0:T(8,128)(2,1)}), bf16[32,16,128]{2,1,0:T(8,128)(2,1)S(1)}, u32[]{:S(2)}, u32[]{:S(2)}) async-start(bf16[32,16,128]{2,1,0:T(8,128)(2,1)} %broadcast_in_dim.10), calls=%async_computation.2 | async-start | bytes 262144 | tf_op jit(solution)/shard_map/all_to_all | solution.py:34
  95.3 0.6 gather_fusion.1
  96.0 9.9 %all-to-all-done.2 = bf16[32,16,128]{2,1,0:T(8,128)(2,1)S(1)} async-done(((bf16[32,16,128]{2,1,0:T(8,128)(2,1)}), bf16[32,16,128]{2,1,0:T(8,128)(2,1)S(1)}, u32[]{:S(2)}, u32[]{:S(2)}) %all-to-all-start.2) | async-done | bytes 131104 | tf_op jit(solution)/shard_map/all_to_all | solution.py:34
  106.0 1.4 %convolution_convert_fusion.1 = bf16[16,64]{1,0:T(8,128)(2,1)S(1)} fusion(bf16[4096,128]{0,1:T(8,128)(2,1)} %all-gather.5.cloned.1.call-done, f32[4096]{0:T(1024)S(1)} %bitcast.356, f32[16]{0:T(128)S(1)} %add_rsqrt_fusion, bf16[32,16,128]{2,1,0:T(8,128)(2,1)S(1)} %all-to-all-done.2), kind=kOutput, calls=%fused_computation.26 | convolution fusion | flops 8651776 | bytes 673856 | tf_op jit(solution)/shard_map/dot_general | solution.py:121
  108.7 0.7 reshape.399
  109.4 3.8 %all-to-all-start.3 = ((bf16[32,2,512]{2,1,0:T(2,128)(2,1)}), bf16[32,2,512]{2,1,0:T(2,128)(2,1)S(1)}, u32[]{:S(2)}, u32[]{:S(2)}) async-start(bf16[32,2,512]{2,1,0:T(2,128)(2,1)} %reshape.399), calls=%async_computation.3 | async-start | bytes 131072 | tf_op jit(solution)/shard_map/all_to_all | solution.py:34
  113.3 0.7 copy.62
  113.9 0.7 copy.61
  114.6 8.7 %all-to-all-done.3 = bf16[32,2,512]{2,1,0:T(2,128)(2,1)S(1)} async-done(((bf16[32,2,512]{2,1,0:T(2,128)(2,1)}), bf16[32,2,512]{2,1,0:T(2,128)(2,1)S(1)}, u32[]{:S(2)}, u32[]{:S(2)}) %all-to-all-start.3) | async-done | bytes 65568 | tf_op jit(solution)/shard_map/all_to_all | solution.py:34
  123.7 0.8 fusion.23
  (139 shorter events, 6.2 us)
Async XLA Ops:
  7.2 57.8 %all-gather.3.cloned.1.call-start = ((), (), s32[]{:S(2)}) async-start(), calls=%async_computation.4 | async-start | bytes 1114112 | tf_op jit(solution)/shard_map/all_gather | solution.py:50
  8.7 0.8 copy-start
  9.5 5.9 %copy-start.8 = (bf16[16,128]{1,0:T(8,128)(2,1)S(1)}, bf16[16,128]{1,0:T(8,128)(2,1)}, u32[]{:S(2)}) copy-start(bf16[16,128]{1,0:T(8,128)(2,1)} %param.15) | copy-start | bytes 12292
  9.5 21.4 %collective-permute-start = (bf16[128,128]{1,0:T(8,128)(2,1)S(1)}, bf16[128,128]{1,0:T(8,128)(2,1)S(1)}, u32[]{:S(2)}, u32[]{:S(2)}) collective-permute-start(bf16[128,128]{1,0:T(8,128)(2,1)S(1)} %get-tuple-element.15), channel_id=1, source_target_pairs={{0,1},{1,2},{2,3},{3,4},{4,5},{5,6},{6,7},{7,8},{8,9},{9,10},{10,1... | collective-permute-start | bytes 98312 | tf_op jit(solution)/shard_map/ppermute | solution.py:23
  9.5 22.0 %collective-permute-start.8 = (bf16[128,128]{1,0:T(8,128)(2,1)S(1)}, bf16[128,128]{1,0:T(8,128)(2,1)S(1)}, u32[]{:S(2)}, u32[]{:S(2)}) collective-permute-start(bf16[128,128]{1,0:T(8,128)(2,1)S(1)} %get-tuple-element.15), channel_id=1, source_target_pairs={{1,0},{2,1},{3,2},{4,3},{5,4},{6,5},{7,6},{8,7},{9,8},{10,9},{11,1... | collective-permute-start | bytes 98312 | tf_op jit(solution)/shard_map/ppermute | solution.py:25
  12.5 18.4 %collective-permute-start.15 = (bf16[128,128]{1,0:T(8,128)(2,1)S(1)}, bf16[128,128]{1,0:T(8,128)(2,1)S(1)}, u32[]{:S(2)}, u32[]{:S(2)}) collective-permute-start(bf16[128,128]{1,0:T(8,128)(2,1)S(1)} %get-tuple-element.14), channel_id=1, source_target_pairs={{0,1},{1,2},{2,3},{3,4},{4,5},{5,6},{6,7},{7,8},{8,9},{9,10},{10,1... | collective-permute-start | bytes 98312 | tf_op jit(solution)/shard_map/ppermute | solution.py:23
  12.5 21.5 %collective-permute-start.23 = (bf16[128,128]{1,0:T(8,128)(2,1)S(1)}, bf16[128,128]{1,0:T(8,128)(2,1)S(1)}, u32[]{:S(2)}, u32[]{:S(2)}) collective-permute-start(bf16[128,128]{1,0:T(8,128)(2,1)S(1)} %get-tuple-element.14), channel_id=1, source_target_pairs={{1,0},{2,1},{3,2},{4,3},{5,4},{6,5},{7,6},{8,7},{9,8},{10,9},{11,1... | collective-permute-start | bytes 98312 | tf_op jit(solution)/shard_map/ppermute | solution.py:25
  16.1 43.4 %all-to-all-start = ((bf16[32,16,128]{2,1,0:T(8,128)(2,1)}), bf16[32,16,128]{2,1,0:T(8,128)(2,1)S(1)}, u32[]{:S(2)}, u32[]{:S(2)}) async-start(bf16[32,16,128]{2,1,0:T(8,128)(2,1)} %broadcast_in_dim.8), calls=%async_computation | async-start | bytes 262144 | tf_op jit(solution)/shard_map/all_to_all | solution.py:34
  29.3 76.7 %all-gather.5.cloned.1.call-start = ((), (), s32[]{:S(2)}) async-start(), calls=%async_computation.5 | async-start | bytes 1114112 | tf_op jit(solution)/shard_map/all_gather | solution.py:50
  30.0 0.8 copy-start.4
  30.0 0.9 copy-start.5
  30.9 5.1 %copy-start.10 = (f32[2,4,64]{2,1,0:T(4,128)S(1)}, f32[2,4,64]{2,1,0:T(4,128)}, u32[]{:S(2)}) copy-start(f32[2,4,64]{2,1,0:T(4,128)} %param.20) | copy-start | bytes 6148
  30.9 5.1 %copy-start.9 = (f32[2,4,64]{2,1,0:T(4,128)S(1)}, f32[2,4,64]{2,1,0:T(4,128)}, u32[]{:S(2)}) copy-start(f32[2,4,64]{2,1,0:T(4,128)} %param.19) | copy-start | bytes 6148
  30.9 4.6 %collective-permute-start.1 = (bf16[128,128]{1,0:T(8,128)(2,1)S(1)}, bf16[128,128]{1,0:T(8,128)(2,1)S(1)}, u32[]{:S(2)}, u32[]{:S(2)}) collective-permute-start(bf16[128,128]{1,0:T(8,128)(2,1)S(1)} %collective-permute-done), channel_id=1, source_target_pairs={{0,1},{1,2},{2,3},{3,4},{4,5},{5,6},{6,7},{7,8},{8,9},{9,10},{10,1... | collective-permute-start | bytes 98312 | tf_op jit(solution)/shard_map/ppermute | solution.py:23
  30.9 5.0 %collective-permute-start.16 = (bf16[128,128]{1,0:T(8,128)(2,1)S(1)}, bf16[128,128]{1,0:T(8,128)(2,1)S(1)}, u32[]{:S(2)}, u32[]{:S(2)}) collective-permute-start(bf16[128,128]{1,0:T(8,128)(2,1)S(1)} %collective-permute-done.15), channel_id=1, source_target_pairs={{0,1},{1,2},{2,3},{3,4},{4,5},{5,6},{6,7},{7,8},{8,9},{9,10},{10,1... | collective-permute-start | bytes 98312 | tf_op jit(solution)/shard_map/ppermute | solution.py:23
  31.5 4.6 %collective-permute-start.9 = (bf16[128,128]{1,0:T(8,128)(2,1)S(1)}, bf16[128,128]{1,0:T(8,128)(2,1)S(1)}, u32[]{:S(2)}, u32[]{:S(2)}) collective-permute-start(bf16[128,128]{1,0:T(8,128)(2,1)S(1)} %collective-permute-done.8), channel_id=1, source_target_pairs={{1,0},{2,1},{3,2},{4,3},{5,4},{6,5},{7,6},{8,7},{9,8},{10,9},{11,1... | collective-permute-start | bytes 98312 | tf_op jit(solution)/shard_map/ppermute | solution.py:25
  33.9 5.1 %collective-permute-start.24 = (bf16[128,128]{1,0:T(8,128)(2,1)S(1)}, bf16[128,128]{1,0:T(8,128)(2,1)S(1)}, u32[]{:S(2)}, u32[]{:S(2)}) collective-permute-start(bf16[128,128]{1,0:T(8,128)(2,1)S(1)} %collective-permute-done.23), channel_id=1, source_target_pairs={{1,0},{2,1},{3,2},{4,3},{5,4},{6,5},{7,6},{8,7},{9,8},{10,9},{11,1... | collective-permute-start | bytes 98312 | tf_op jit(solution)/shard_map/ppermute | solution.py:25
  35.5 4.8 %collective-permute-start.2 = (bf16[128,128]{1,0:T(8,128)(2,1)S(1)}, bf16[128,128]{1,0:T(8,128)(2,1)S(1)}, u32[]{:S(2)}, u32[]{:S(2)}) collective-permute-start(bf16[128,128]{1,0:T(8,128)(2,1)S(1)} %collective-permute-done.1), channel_id=1, source_target_pairs={{0,1},{1,2},{2,3},{3,4},{4,5},{5,6},{6,7},{7,8},{8,9},{9,10},{10,1... | collective-permute-start | bytes 98312 | tf_op jit(solution)/shard_map/ppermute | solution.py:23
  35.9 5.1 %collective-permute-start.17 = (bf16[128,128]{1,0:T(8,128)(2,1)S(1)}, bf16[128,128]{1,0:T(8,128)(2,1)S(1)}, u32[]{:S(2)}, u32[]{:S(2)}) collective-permute-start(bf16[128,128]{1,0:T(8,128)(2,1)S(1)} %collective-permute-done.16), channel_id=1, source_target_pairs={{0,1},{1,2},{2,3},{3,4},{4,5},{5,6},{6,7},{7,8},{8,9},{9,10},{10,1... | collective-permute-start | bytes 98312 | tf_op jit(solution)/shard_map/ppermute | solution.py:23
  36.1 9.5 %copy-start.11 = (f32[2,4,16]{2,1,0:T(4,128)S(1)}, f32[2,4,16]{2,1,0:T(4,128)}, u32[]{:S(2)}) copy-start(f32[2,4,16]{2,1,0:T(4,128)} %param.26) | copy-start | bytes 1540
  36.1 5.1 %collective-permute-start.10 = (bf16[128,128]{1,0:T(8,128)(2,1)S(1)}, bf16[128,128]{1,0:T(8,128)(2,1)S(1)}, u32[]{:S(2)}, u32[]{:S(2)}) collective-permute-start(bf16[128,128]{1,0:T(8,128)(2,1)S(1)} %collective-permute-done.9), channel_id=1, source_target_pairs={{1,0},{2,1},{3,2},{4,3},{5,4},{6,5},{7,6},{8,7},{9,8},{10,9},{11,1... | collective-permute-start | bytes 98312 | tf_op jit(solution)/shard_map/ppermute | solution.py:25
  39.1 5.1 %collective-permute-start.25 = (bf16[128,128]{1,0:T(8,128)(2,1)S(1)}, bf16[128,128]{1,0:T(8,128)(2,1)S(1)}, u32[]{:S(2)}, u32[]{:S(2)}) collective-permute-start(bf16[128,128]{1,0:T(8,128)(2,1)S(1)} %collective-permute-done.24), channel_id=1, source_target_pairs={{1,0},{2,1},{3,2},{4,3},{5,4},{6,5},{7,6},{8,7},{9,8},{10,9},{11,1... | collective-permute-start | bytes 98312 | tf_op jit(solution)/shard_map/ppermute | solution.py:25
  40.2 4.6 %collective-permute-start.3 = (bf16[128,128]{1,0:T(8,128)(2,1)S(1)}, bf16[128,128]{1,0:T(8,128)(2,1)S(1)}, u32[]{:S(2)}, u32[]{:S(2)}) collective-permute-start(bf16[128,128]{1,0:T(8,128)(2,1)S(1)} %collective-permute-done.2), channel_id=1, source_target_pairs={{0,1},{1,2},{2,3},{3,4},{4,5},{5,6},{6,7},{7,8},{8,9},{9,10},{10,1... | collective-permute-start | bytes 98312 | tf_op jit(solution)/shard_map/ppermute | solution.py:23
  41.1 4.6 %collective-permute-start.18 = (bf16[128,128]{1,0:T(8,128)(2,1)S(1)}, bf16[128,128]{1,0:T(8,128)(2,1)S(1)}, u32[]{:S(2)}, u32[]{:S(2)}) collective-permute-start(bf16[128,128]{1,0:T(8,128)(2,1)S(1)} %collective-permute-done.17), channel_id=1, source_target_pairs={{0,1},{1,2},{2,3},{3,4},{4,5},{5,6},{6,7},{7,8},{8,9},{9,10},{10,1... | collective-permute-start | bytes 98312 | tf_op jit(solution)/shard_map/ppermute | solution.py:23
  41.2 4.7 %collective-permute-start.11 = (bf16[128,128]{1,0:T(8,128)(2,1)S(1)}, bf16[128,128]{1,0:T(8,128)(2,1)S(1)}, u32[]{:S(2)}, u32[]{:S(2)}) collective-permute-start(bf16[128,128]{1,0:T(8,128)(2,1)S(1)} %collective-permute-done.10), channel_id=1, source_target_pairs={{1,0},{2,1},{3,2},{4,3},{5,4},{6,5},{7,6},{8,7},{9,8},{10,9},{11,1... | collective-permute-start | bytes 98312 | tf_op jit(solution)/shard_map/ppermute | solution.py:25
  44.2 5.3 %collective-permute-start.26 = (bf16[128,128]{1,0:T(8,128)(2,1)S(1)}, bf16[128,128]{1,0:T(8,128)(2,1)S(1)}, u32[]{:S(2)}, u32[]{:S(2)}) collective-permute-start(bf16[128,128]{1,0:T(8,128)(2,1)S(1)} %collective-permute-done.25), channel_id=1, source_target_pairs={{1,0},{2,1},{3,2},{4,3},{5,4},{6,5},{7,6},{8,7},{9,8},{10,9},{11,1... | collective-permute-start | bytes 98312 | tf_op jit(solution)/shard_map/ppermute | solution.py:25
  44.8 5.3 %collective-permute-start.4 = (bf16[128,128]{1,0:T(8,128)(2,1)S(1)}, bf16[128,128]{1,0:T(8,128)(2,1)S(1)}, u32[]{:S(2)}, u32[]{:S(2)}) collective-permute-start(bf16[128,128]{1,0:T(8,128)(2,1)S(1)} %collective-permute-done.3), channel_id=1, source_target_pairs={{0,1},{1,2},{2,3},{3,4},{4,5},{5,6},{6,7},{7,8},{8,9},{9,10},{10,1... | collective-permute-start | bytes 98312 | tf_op jit(solution)/shard_map/ppermute | solution.py:23
  45.6 4.6 %collective-permute-start.19 = (bf16[128,128]{1,0:T(8,128)(2,1)S(1)}, bf16[128,128]{1,0:T(8,128)(2,1)S(1)}, u32[]{:S(2)}, u32[]{:S(2)}) collective-permute-start(bf16[128,128]{1,0:T(8,128)(2,1)S(1)} %collective-permute-done.18), channel_id=1, source_target_pairs={{0,1},{1,2},{2,3},{3,4},{4,5},{5,6},{6,7},{7,8},{8,9},{9,10},{10,1... | collective-permute-start | bytes 98312 | tf_op jit(solution)/shard_map/ppermute | solution.py:23
  45.9 5.1 %collective-permute-start.12 = (bf16[128,128]{1,0:T(8,128)(2,1)S(1)}, bf16[128,128]{1,0:T(8,128)(2,1)S(1)}, u32[]{:S(2)}, u32[]{:S(2)}) collective-permute-start(bf16[128,128]{1,0:T(8,128)(2,1)S(1)} %collective-permute-done.11), channel_id=1, source_target_pairs={{1,0},{2,1},{3,2},{4,3},{5,4},{6,5},{7,6},{8,7},{9,8},{10,9},{11,1... | collective-permute-start | bytes 98312 | tf_op jit(solution)/shard_map/ppermute | solution.py:25
  49.5 4.6 %collective-permute-start.27 = (bf16[128,128]{1,0:T(8,128)(2,1)S(1)}, bf16[128,128]{1,0:T(8,128)(2,1)S(1)}, u32[]{:S(2)}, u32[]{:S(2)}) collective-permute-start(bf16[128,128]{1,0:T(8,128)(2,1)S(1)} %collective-permute-done.26), channel_id=1, source_target_pairs={{1,0},{2,1},{3,2},{4,3},{5,4},{6,5},{7,6},{8,7},{9,8},{10,9},{11,1... | collective-permute-start | bytes 98312 | tf_op jit(solution)/shard_map/ppermute | solution.py:25
  50.0 4.6 %collective-permute-start.5 = (bf16[128,128]{1,0:T(8,128)(2,1)S(1)}, bf16[128,128]{1,0:T(8,128)(2,1)S(1)}, u32[]{:S(2)}, u32[]{:S(2)}) collective-permute-start(bf16[128,128]{1,0:T(8,128)(2,1)S(1)} %collective-permute-done.4), channel_id=1, source_target_pairs={{0,1},{1,2},{2,3},{3,4},{4,5},{5,6},{6,7},{7,8},{8,9},{9,10},{10,1... | collective-permute-start | bytes 98312 | tf_op jit(solution)/shard_map/ppermute | solution.py:23
  50.2 4.8 %collective-permute-start.20 = (bf16[128,128]{1,0:T(8,128)(2,1)S(1)}, bf16[128,128]{1,0:T(8,128)(2,1)S(1)}, u32[]{:S(2)}, u32[]{:S(2)}) collective-permute-start(bf16[128,128]{1,0:T(8,128)(2,1)S(1)} %collective-permute-done.19), channel_id=1, source_target_pairs={{0,1},{1,2},{2,3},{3,4},{4,5},{5,6},{6,7},{7,8},{8,9},{9,10},{10,1... | collective-permute-start | bytes 98312 | tf_op jit(solution)/shard_map/ppermute | solution.py:23
  51.0 4.6 %collective-permute-start.13 = (bf16[128,128]{1,0:T(8,128)(2,1)S(1)}, bf16[128,128]{1,0:T(8,128)(2,1)S(1)}, u32[]{:S(2)}, u32[]{:S(2)}) collective-permute-start(bf16[128,128]{1,0:T(8,128)(2,1)S(1)} %collective-permute-done.12), channel_id=1, source_target_pairs={{1,0},{2,1},{3,2},{4,3},{5,4},{6,5},{7,6},{8,7},{9,8},{10,9},{11,1... | collective-permute-start | bytes 98312 | tf_op jit(solution)/shard_map/ppermute | solution.py:25
  54.0 4.6 %collective-permute-start.28 = (bf16[128,128]{1,0:T(8,128)(2,1)S(1)}, bf16[128,128]{1,0:T(8,128)(2,1)S(1)}, u32[]{:S(2)}, u32[]{:S(2)}) collective-permute-start(bf16[128,128]{1,0:T(8,128)(2,1)S(1)} %collective-permute-done.27), channel_id=1, source_target_pairs={{1,0},{2,1},{3,2},{4,3},{5,4},{6,5},{7,6},{8,7},{9,8},{10,9},{11,1... | collective-permute-start | bytes 98312 | tf_op jit(solution)/shard_map/ppermute | solution.py:25
  54.6 4.6 %collective-permute-start.6 = (bf16[128,128]{1,0:T(8,128)(2,1)S(1)}, bf16[128,128]{1,0:T(8,128)(2,1)S(1)}, u32[]{:S(2)}, u32[]{:S(2)}) collective-permute-start(bf16[128,128]{1,0:T(8,128)(2,1)S(1)} %collective-permute-done.5), channel_id=1, source_target_pairs={{0,1},{1,2},{2,3},{3,4},{4,5},{5,6},{6,7},{7,8},{8,9},{9,10},{10,1... | collective-permute-start | bytes 98312 | tf_op jit(solution)/shard_map/ppermute | solution.py:23
  54.9 4.6 %collective-permute-start.21 = (bf16[128,128]{1,0:T(8,128)(2,1)S(1)}, bf16[128,128]{1,0:T(8,128)(2,1)S(1)}, u32[]{:S(2)}, u32[]{:S(2)}) collective-permute-start(bf16[128,128]{1,0:T(8,128)(2,1)S(1)} %collective-permute-done.20), channel_id=1, source_target_pairs={{0,1},{1,2},{2,3},{3,4},{4,5},{5,6},{6,7},{7,8},{8,9},{9,10},{10,1... | collective-permute-start | bytes 98312 | tf_op jit(solution)/shard_map/ppermute | solution.py:23
  55.6 8.6 %collective-permute-start.14 = (bf16[128,128]{1,0:T(8,128)(2,1)S(1)}, bf16[128,128]{1,0:T(8,128)(2,1)S(1)}, u32[]{:S(2)}, u32[]{:S(2)}) collective-permute-start(bf16[128,128]{1,0:T(8,128)(2,1)S(1)} %collective-permute-done.13), channel_id=1, source_target_pairs={{1,0},{2,1},{3,2},{4,3},{5,4},{6,5},{7,6},{8,7},{9,8},{10,9},{11,1... | collective-permute-start | bytes 98312 | tf_op jit(solution)/shard_map/ppermute | solution.py:25
  58.6 36.7 %collective-permute-start.29 = (bf16[128,128]{1,0:T(8,128)(2,1)S(1)}, bf16[128,128]{1,0:T(8,128)(2,1)S(1)}, u32[]{:S(2)}, u32[]{:S(2)}) collective-permute-start(bf16[128,128]{1,0:T(8,128)(2,1)S(1)} %collective-permute-done.28), channel_id=1, source_target_pairs={{1,0},{2,1},{3,2},{4,3},{5,4},{6,5},{7,6},{8,7},{9,8},{10,9},{11,1... | collective-permute-start | bytes 98312 | tf_op jit(solution)/shard_map/ppermute | solution.py:25
  59.1 4.6 %collective-permute-start.7 = (bf16[128,128]{1,0:T(8,128)(2,1)S(1)}, bf16[128,128]{1,0:T(8,128)(2,1)S(1)}, u32[]{:S(2)}, u32[]{:S(2)}) collective-permute-start(bf16[128,128]{1,0:T(8,128)(2,1)S(1)} %collective-permute-done.6), channel_id=1, source_target_pairs={{0,1},{1,2},{2,3},{3,4},{4,5},{5,6},{6,7},{7,8},{8,9},{9,10},{10,1... | collective-permute-start | bytes 98312 | tf_op jit(solution)/shard_map/ppermute | solution.py:23
  59.5 4.6 %collective-permute-start.22 = (bf16[128,128]{1,0:T(8,128)(2,1)S(1)}, bf16[128,128]{1,0:T(8,128)(2,1)S(1)}, u32[]{:S(2)}, u32[]{:S(2)}) collective-permute-start(bf16[128,128]{1,0:T(8,128)(2,1)S(1)} %collective-permute-done.21), channel_id=1, source_target_pairs={{0,1},{1,2},{2,3},{3,4},{4,5},{5,6},{6,7},{7,8},{8,9},{9,10},{10,1... | collective-permute-start | bytes 98312 | tf_op jit(solution)/shard_map/ppermute | solution.py:23
  65.0 1.5 %copy-start.1 = (f32[2,4,16,64]{3,2,1,0:T(8,128)S(1)}, f32[2,4,16,64]{3,2,1,0:T(8,128)}, u32[]{:S(2)}) copy-start(f32[2,4,16,64]{3,2,1,0:T(8,128)} %param.23) | copy-start | bytes 98308
  65.0 1.5 %copy-start.2 = (f32[2,4,16,64]{3,2,1,0:T(8,128)S(1)}, f32[2,4,16,64]{3,2,1,0:T(8,128)}, u32[]{:S(2)}) copy-start(f32[2,4,16,64]{3,2,1,0:T(8,128)} %param.22) | copy-start | bytes 98308
  66.5 0.8 copy-start.3
  67.5 0.8 copy-start.6
  70.8 19.3 %all-to-all-start.1 = ((bf16[32,2,512]{2,1,0:T(2,128)(2,1)}), bf16[32,2,512]{2,1,0:T(2,128)(2,1)S(1)}, u32[]{:S(2)}, u32[]{:S(2)}) async-start(bf16[32,2,512]{2,1,0:T(2,128)(2,1)} %reshape.397), calls=%async_computation.1 | async-start | bytes 131072 | tf_op jit(solution)/shard_map/all_to_all | solution.py:34
  91.4 14.4 %all-to-all-start.2 = ((bf16[32,16,128]{2,1,0:T(8,128)(2,1)}), bf16[32,16,128]{2,1,0:T(8,128)(2,1)S(1)}, u32[]{:S(2)}, u32[]{:S(2)}) async-start(bf16[32,16,128]{2,1,0:T(8,128)(2,1)} %broadcast_in_dim.10), calls=%async_computation.2 | async-start | bytes 262144 | tf_op jit(solution)/shard_map/all_to_all | solution.py:34
  106.0 2.3 %copy-start.13 = (bf16[4096,128]{0,1:T(8,128)(2,1)S(1)}, bf16[4096,128]{0,1:T(8,128)(2,1)}, u32[]{:S(2)}) copy-start(bf16[4096,128]{0,1:T(8,128)(2,1)} %all-gather.5.cloned.1.call-done) | copy-start | bytes 3145732
  109.4 13.9 %all-to-all-start.3 = ((bf16[32,2,512]{2,1,0:T(2,128)(2,1)}), bf16[32,2,512]{2,1,0:T(2,128)(2,1)S(1)}, u32[]{:S(2)}, u32[]{:S(2)}) async-start(bf16[32,2,512]{2,1,0:T(2,128)(2,1)} %reshape.399), calls=%async_computation.3 | async-start | bytes 131072 | tf_op jit(solution)/shard_map/all_to_all | solution.py:34
  (2 other events, 1.4 us)
Sparse Core Ops, SparseCore 0:
  10.6 42.7 all-gather.2
  56.0 39.8 all-gather.4
